TPU v7x, 32 devices: a whole 2x2x4 slice. The times are simulated.
32 devices in a mesh: ep: 8 (over z, x), tp: 4 (over y, core).
Axes of the slice: x: 2, y: 2, z: 4, core: 2. Of those that a mesh axis runs over, the one named last changes fastest.
Arguments:
- query_rows: bfloat16 [3072, 1024], P('ep', 'tp'), may hold values from -8 to 8
- key_rows: bfloat16 [3072, 256], P('ep'), may hold values from -8 to 8
- value_rows: bfloat16 [3072, 256], P('ep'), may hold values from -6 to 6
- query_gain: float32 [64], replicated, may hold values from 0.3 to 6
- key_gain: float32 [64], replicated, may hold values from 0.3 to 6
- out_weight: bfloat16 [1024, 2048], P('tp'), may hold values from -0.1875 to 0.1875
- mixer_gain: float32 [2048], replicated, may hold values from 0.1 to 1.9
- expert_input: bfloat16 [2048, 2048], P('ep'), may hold values from -6 to 6
- expert_ids: int32 [2048, 2], P('ep'), may hold values from 0 to 7, all different within a row; in each aligned block of 256 rows (0 to 255, 256 to 511, ...) at most 96 rows name the same one
- gate_score: float32 [2048, 2], P('ep'), may hold values from 0.05 to 1
- expert_gain: float32 [2048], replicated, may hold values from 0.1 to 1.9
- gate_weight: bfloat16 [8, 2048, 4096], P('ep', None, 'tp'), may hold values from -0.125 to 0.125
- up_weight: bfloat16 [8, 2048, 4096], P('ep', None, 'tp'), may hold values from -0.125 to 0.125
- down_weight: bfloat16 [8, 4096, 2048], P('ep', 'tp'), may hold values from -0.09375 to 0.09375
- shared_gate: bfloat16 [2048, 2048], P(None, 'tp'), may hold values from -0.125 to 0.125
- shared_up: bfloat16 [2048, 2048], P(None, 'tp'), may hold values from -0.125 to 0.125
- shared_down: bfloat16 [2048, 2048], P('tp'), may hold values from -0.125 to 0.125
Outputs:
- mixer_out: bfloat16 [3072, 2048], P('ep')
- expert_out: bfloat16 [2048, 2048], P('ep', 'tp')
Inputs may be any that keep to these rules, and one draw needn't show every extreme that they name: `expert_ids`: each row names 2 different experts. In each aligned block of 256 rows (the rows of one device) no expert is named by more than 96 rows, a bound that some block reaches.
All inputs are finite; a program needn't handle non-finite values.
Results may differ from a plain program's by a relative error of at most 0.02.
The roundings to bfloat16 on the way count: a program that leaves them out, or rounds other values in their place, can miss the bound.
Values may be sent and summed in bfloat16 or wider, within the bound.
A program may use at most 128 MiB of HBM per device.

v0:
```python
import math
import jax
import jax.numpy as jnp
from jax import lax
from jax.sharding import PartitionSpec as P

HEADS = 16
KV_HEADS = 4
HEAD_DIM = 64
GRID_W = 64
EPSILON = 1e-06
ROUTED_SCALE = 2.5


def rotary_angles(position):
    grid_row = (position // GRID_W).astype(jnp.float32)
    grid_col = (position % GRID_W).astype(jnp.float32)
    quarter = HEAD_DIM // 4
    inverse = 10000.0 ** (-jnp.arange(quarter, dtype=jnp.float32) / quarter)
    return jnp.concatenate([grid_row[:, None] * inverse, grid_col[:, None] * inverse], axis=1)


def normalize_rotate(heads_in, gain_vector, angles):
    widened = heads_in.astype(jnp.float32)
    scaled = widened * lax.rsqrt(jnp.mean(widened * widened, axis=-1, keepdims=True) + EPSILON)
    scaled = scaled * gain_vector
    half_dim = scaled.shape[-1] // 2
    front_half = scaled[..., :half_dim]
    back_half = scaled[..., half_dim:]
    cosine_table = jnp.cos(angles)[:, None, :]
    sine_table = jnp.sin(angles)[:, None, :]
    turned = jnp.concatenate(
        [
            front_half * cosine_table - back_half * sine_table,
            front_half * sine_table + back_half * cosine_table,
        ],
        axis=-1,
    )
    return turned.astype(jnp.bfloat16)


def mixer_half(query_rows, key_rows, value_rows, query_gain, key_gain, out_weight, mixer_gain):
    local_rows = query_rows.shape[0]
    lane_heads = query_rows.shape[1] // HEAD_DIM
    group = HEADS // KV_HEADS
    lane_kv = max(1, lane_heads // group)
    local_group = lane_heads // lane_kv
    first_kv = lax.axis_index("tp") * lane_heads // group
    offset = lax.axis_index("ep") * local_rows
    angles = rotary_angles(offset + jnp.arange(local_rows, dtype=jnp.int32))
    query_rot = normalize_rotate(
        query_rows.reshape(local_rows, lane_heads, HEAD_DIM), query_gain, angles
    )
    query_grouped = query_rot.reshape(local_rows, lane_kv, local_group, HEAD_DIM)
    key_cols = lax.dynamic_slice_in_dim(key_rows, first_kv * HEAD_DIM, lane_kv * HEAD_DIM, 1)
    value_cols = lax.dynamic_slice_in_dim(value_rows, first_kv * HEAD_DIM, lane_kv * HEAD_DIM, 1)
    key_rot = normalize_rotate(key_cols.reshape(local_rows, lane_kv, HEAD_DIM), key_gain, angles)
    stacked = jnp.concatenate([key_rot.reshape(local_rows, lane_kv * HEAD_DIM), value_cols], axis=1)
    scale_factor = HEAD_DIM ** (-0.5)
    key_width = lane_kv * HEAD_DIM

    def step_block(state, block_rows):
        row_peak, row_total, accum = state
        block_keys = block_rows[:, :key_width].reshape(block_rows.shape[0], lane_kv, HEAD_DIM)
        block_values = block_rows[:, key_width:].reshape(block_rows.shape[0], lane_kv, HEAD_DIM)
        scores = (
            jnp.einsum(
                "qkgd,skd->kgqs", query_grouped, block_keys, preferred_element_type=jnp.float32
            )
            * scale_factor
        )
        new_peak = jnp.maximum(row_peak, jnp.max(scores, axis=3))
        shrink = jnp.exp(row_peak - new_peak)
        exponent = jnp.exp(scores - new_peak[..., None])
        row_total = row_total * shrink + jnp.sum(exponent, axis=3)
        accum = accum * shrink[..., None] + jnp.einsum(
            "kgqs,skd->kgqd",
            exponent.astype(jnp.bfloat16),
            block_values,
            preferred_element_type=jnp.float32,
        )
        return ((new_peak, row_total, accum), None)

    start_state = (
        jnp.full((lane_kv, local_group, local_rows), -jnp.inf, jnp.float32),
        jnp.zeros((lane_kv, local_group, local_rows), jnp.float32),
        jnp.zeros((lane_kv, local_group, local_rows, HEAD_DIM), jnp.float32),
    )
    carry = start_state
    piece = lax.all_gather(stacked, "ep", axis=0, tiled=True)
    shard_count = piece.shape[0] // local_rows
    per_block = math.gcd(shard_count, max(1, 2048 // local_rows))
    block_rows = per_block * local_rows
    blocks = piece.reshape(piece.shape[0] // block_rows, block_rows, piece.shape[1])
    carry, unused = lax.scan(step_block, carry, blocks)
    row_peak, row_total, accum = carry
    attended = (accum / row_total[..., None]).astype(jnp.bfloat16)
    lane_weight = out_weight.reshape(lane_kv, local_group, HEAD_DIM, out_weight.shape[1])
    partial_value = jnp.einsum(
        "kgqd,kgde->qe", attended, lane_weight, preferred_element_type=jnp.float32
    )
    mixer_sum = lax.psum(partial_value.astype(jnp.bfloat16), "tp").astype(jnp.float32)
    mixer_scale = lax.rsqrt(jnp.mean(mixer_sum * mixer_sum, axis=1, keepdims=True) + EPSILON)
    return (mixer_sum * mixer_scale * mixer_gain).astype(jnp.bfloat16)


def expert_half(
    expert_input,
    expert_ids,
    gate_score,
    expert_gain,
    gate_weight,
    up_weight,
    down_weight,
    shared_gate,
    shared_up,
    shared_down,
):
    local_rows, top_count = expert_ids.shape
    local_experts = gate_weight.shape[0]
    ep_size = lax.axis_size("ep")
    experts_all = local_experts * ep_size
    capacity = 3 * local_rows * top_count // (2 * experts_all)
    model_width = expert_input.shape[1]
    lane_cols = model_width // lax.axis_size("tp")
    slots_total = ep_size * capacity
    widened = expert_input.astype(jnp.float32)
    normed = (
        widened
        * lax.rsqrt(jnp.mean(widened * widened, axis=1, keepdims=True) + EPSILON)
        * expert_gain
    ).astype(jnp.bfloat16)
    route_weight = gate_score / jnp.sum(gate_score, axis=1, keepdims=True) * ROUTED_SCALE
    pair_ids = expert_ids.reshape(local_rows * top_count)
    onehot = (pair_ids[:, None] == jnp.arange(experts_all, dtype=jnp.int32)).astype(jnp.int32)
    ranks = jnp.sum(
        (jnp.cumsum(onehot, axis=0, dtype=jnp.int32) - 1) * onehot, axis=1, dtype=jnp.int32
    )
    slot_index = pair_ids * capacity + ranks
    row_numbers = jnp.arange(local_rows * top_count, dtype=jnp.int32) // top_count
    sources = jnp.full((experts_all * capacity,), -1, jnp.int32).at[slot_index].set(row_numbers)
    filled = (sources >= 0)[:, None]
    safe_rows = jnp.maximum(sources, 0)
    nothing = jnp.zeros((), jnp.bfloat16)
    lane_start = lax.axis_index("tp") * lane_cols
    own_cols = lax.dynamic_slice_in_dim(normed, lane_start, lane_cols, 1)
    outgoing = jnp.where(filled, own_cols[safe_rows], nothing).reshape(
        experts_all, capacity, lane_cols
    )
    arrived = lax.all_to_all(outgoing, "ep", split_axis=0, concat_axis=0, tiled=True)
    arranged = arrived.reshape(ep_size, local_experts, capacity, lane_cols).transpose(1, 0, 2, 3)
    arranged = arranged.reshape(local_experts, slots_total, lane_cols)
    piece = lax.all_gather(arranged, "tp", axis=2, tiled=True)
    gate_value = jnp.einsum("esd,edf->esf", piece, gate_weight, preferred_element_type=jnp.float32)
    up_value = jnp.einsum("esd,edf->esf", piece, up_weight, preferred_element_type=jnp.float32)
    hidden = (jax.nn.silu(gate_value) * up_value).astype(jnp.bfloat16)
    down_part = jnp.einsum("esf,efd->esd", hidden, down_weight, preferred_element_type=jnp.float32)
    down_rows = down_part.reshape(local_experts, ep_size, capacity, model_width).transpose(
        1, 0, 2, 3
    )
    down_rows = down_rows.reshape(experts_all * capacity, model_width)
    shared_gate_value = jnp.dot(normed, shared_gate, preferred_element_type=jnp.float32)
    shared_up_value = jnp.dot(normed, shared_up, preferred_element_type=jnp.float32)
    shared_hidden = (jax.nn.silu(shared_gate_value) * shared_up_value).astype(jnp.bfloat16)
    shared_part = jnp.dot(shared_hidden, shared_down, preferred_element_type=jnp.float32)
    terms = jnp.concatenate([down_rows, shared_part], axis=0)
    summed = lax.psum_scatter(
        terms.astype(jnp.bfloat16), "tp", scatter_dimension=1, tiled=True
    ).astype(jnp.float32)
    routed_slots = (
        summed[: experts_all * capacity]
        .astype(jnp.bfloat16)
        .reshape(experts_all, capacity, lane_cols)
    )
    shared_cols = summed[experts_all * capacity :]
    returned = lax.all_to_all(routed_slots, "ep", split_axis=0, concat_axis=0, tiled=True)
    picked = returned.reshape(experts_all * capacity, lane_cols)[slot_index]
    picked = picked.reshape(local_rows, top_count, lane_cols)
    routed = jnp.sum(picked.astype(jnp.float32) * route_weight[:, :, None], axis=1)
    return (routed + shared_cols).astype(jnp.bfloat16)


def body(
    query_rows,
    key_rows,
    value_rows,
    query_gain,
    key_gain,
    out_weight,
    mixer_gain,
    expert_input,
    expert_ids,
    gate_score,
    expert_gain,
    gate_weight,
    up_weight,
    down_weight,
    shared_gate,
    shared_up,
    shared_down,
):
    mixer_out = mixer_half(
        query_rows, key_rows, value_rows, query_gain, key_gain, out_weight, mixer_gain
    )
    expert_out = expert_half(
        expert_input,
        expert_ids,
        gate_score,
        expert_gain,
        gate_weight,
        up_weight,
        down_weight,
        shared_gate,
        shared_up,
        shared_down,
    )
    return (mixer_out, expert_out)


def solution(mesh):
    in_specs = (
        P("ep", "tp"),
        P("ep", None),
        P("ep", None),
        P(),
        P(),
        P("tp", None),
        P(),
        P("ep", None),
        P("ep", None),
        P("ep", None),
        P(),
        P("ep", None, "tp"),
        P("ep", None, "tp"),
        P("ep", "tp", None),
        P(None, "tp"),
        P(None, "tp"),
        P("tp", None),
    )
    out_specs = (P("ep", None), P("ep", "tp"))
    return jax.shard_map(body, mesh=mesh, in_specs=in_specs, out_specs=out_specs, check_vma=False)
```

profile of v0, /device:TPU:0, one launch (start us, length us, event | category | flops | bytes accessed | tf_op | source)
XLA Modules:
  0.0 218.4 jit_solution(9273533455983463291)
XLA Ops:
  11.0 2.4 %scatter_custom_fusion = s32[768]{0:T(1024)S(1)} fusion(s32[512]{0:T(512)S(1)} %bitcast.141, s32[512]{0:T(512)S(1)} %add_select_fusion, s32[]{:T(128)} %constant.116.clone.1), kind=kCustom, calls=%fused_computation.114 | custom fusion | bytes 3076 | tf_op jit(solution)/shard_map/scatter | solution.py:141
  17.1 2.7 %gather_fusion = bf16[768,512]{1,0:T(8,128)(2,1)S(1)} fusion(bf16[256,512]{1,0:T(8,128)(2,1)S(1)} %constant_dynamic-slice_fusion.1, s32[1024]{0:T(1024)S(1)} %pad_clamp_fusion.1), kind=kCustom, calls=%fused_computation | custom fusion | bytes 1575936 | tf_op jit(solution)/shard_map/gather | solution.py:147
  20.0 27.3 %all_to_all.10 = bf16[8,96,512]{2,1,0:T(8,128)(2,1)} all-to-all(bf16[8,96,512]{2,1,0:T(8,128)(2,1)S(1)} %broadcast_select_fusion), channel_id=1, replica_groups=mesh['ep'=8,'tp'=4] {'ep'}, dimensions={0} | all-to-all | bytes 1572864 | tf_op jit(solution)/shard_map/all_to_all | solution.py:150
  50.8 3.1 %fusion.67 = f32[256,512]{1,0:T(8,128)} fusion(bf16[256,2048]{1,0:T(8,128)(2,1)S(1)} %copy-done.5, bf16[2048,512]{1,0:T(8,128)(2,1)} %param.33), kind=kOutput, calls=%fused_computation.131 | convolution fusion | flops 536870912 | bytes 3670016 | tf_op jit(solution)/shard_map/dot_general | solution.py:162
  53.9 34.3 %all_gather.6 = bf16[3072,128]{1,0:T(8,128)(2,1)} all-gather(bf16[384,128]{1,0:T(8,128)(2,1)S(1)} %pad_maximum_fusion.2), channel_id=1, replica_groups=mesh['ep'=8,'tp'=4] {'ep'}, dimensions={0}, use_global_device_ids=true | all-gather | bytes 884736 | tf_op jit(solution)/shard_map/all_gather | solution.py:90
  88.1 4.3 %convolution_convert_fusion = bf16[256,2048]{1,0:T(8,128)(2,1)} fusion(bf16[512,2048]{1,0:T(8,128)(2,1)S(1)} %copy-done, bf16[256,2048]{1,0:T(8,128)(2,1)} %copy-done.4, bf16[2048,512]{1,0:T(8,128)(2,1)} %param.34, f32[256,512]{1,0:T(8,128)} %fusion.67), kind=kOutput, calls=%fused_computation.44 | convolution fusion | flops 1075052544 | bytes 6815744 | tf_op jit(solution)/shard_map/dot_general | solution.py:165
  92.5 6.3 %fusion.16 = f32[768,1024]{1,0:T(8,128)S(1)} fusion(bf16[1,2048,1024]{2,1,0:T(8,128)(2,1)} %param.30, bf16[1,768,2048]{2,1,0:T(8,128)(2,1)} %all-gather.2.cloned.1.call-done), kind=kOutput, calls=%fused_computation.30 | convolution fusion | flops 3221225472 | bytes 10485760 | tf_op jit(solution)/shard_map/esd,edf->esf/dot_general | solution.py:154
  98.8 3.6 %multiply_convert_fusion = bf16[768,1024]{1,0:T(8,128)(2,1)S(1)} fusion(f32[768,1024]{1,0:T(8,128)S(1)} %fusion.16, bf16[1,2048,1024]{2,1,0:T(8,128)(2,1)S(1)} %copy-done.12, bf16[1,768,2048]{2,1,0:T(8,128)(2,1)S(1)} %copy-done.14), kind=kOutput, calls=%fused_computation.41 | convolution fusion | flops 3225944064 | bytes 12058624 | tf_op jit(solution)/shard_map/esd,edf->esf/dot_general | solution.py:155
  102.4 3.6 %fusion.18 = bf16[768,2048]{1,0:T(8,128)(2,1)S(1)} fusion(bf16[768,1024]{1,0:T(8,128)(2,1)S(1)} %multiply_convert_fusion, bf16[1,1024,2048]{2,1,0:T(8,128)(2,1)S(1)} %copy-done.13), kind=kOutput, calls=%fused_computation.34 | convolution fusion | flops 3222798336 | bytes 8912896 | tf_op jit(solution)/shard_map/esf,efd->esd/dot_general | solution.py:157
  106.1 2.2 %pad_maximum_fusion = bf16[1024,2048]{1,0:T(8,128)(2,1)} fusion(bf16[256,2048]{1,0:T(8,128)(2,1)S(1)} %copy-done.6, bf16[768,2048]{1,0:T(8,128)(2,1)S(1)} %fusion.18), kind=kLoop, calls=%fused_computation.25 | loop fusion | flops 8388608 | bytes 8388608 | tf_op jit(solution)/shard_map/concatenate | solution.py:166
  108.4 47.6 %while.15 = (s32[]{:T(128)}, f32[1,4,384]{2,1,0:T(4,128)S(1)}, f32[1,4,384]{2,1,0:T(4,128)S(1)}, f32[1,4,384,64]{2,3,1,0:T(8,128)S(1)}, bf16[8,384,128]{2,1,0:T(...) while((s32[]{:T(128)}, f32[1,4,384]{2,1,0:T(4,128)S(1)}, ...), condition=%wide.region_5.6_spmd.clone, body=%wide.region_2.5_spmd.clone.sunk | while | flops 156017664 | bytes 18088064 | solution.py:95
  109.4 1.9 bitcast_reduce_fusion.2
  111.3 2.8 %fusion.82 = f32[1,4,384,64]{2,3,1,0:T(8,128)S(1)} fusion(f32[384,384,4]{1,0,2:T(8,128)} %get-tuple-element.151, f32[4,384]{1,0:T(4,128)S(1)} %bitcast.134, f32[1,4,384,64]{2,3,1,0:T(8,128)S(1)} %get-tuple-element.164, f32[4,384]{1,0:T(4,128)S(1)} %get-tuple-element.152, pred[]{:T(512)S(6)} %compare.18, bf16[384,128]{0,1:T(8,128)(2,1)S(1)} %bitcast.133), kind=kOutput, calls=%fused_computation.9.clone.1 | convolution fusion | flops 77561856 | bytes 3207169 | tf_op jit(solution)/shard_map/while/body/eval_jaxpr/kgqs,skd->kgqd/dot_general | solution.py:76
  115.9 1.9 bitcast_reduce_fusion.2
  117.8 2.5 %fusion.82 = f32[1,4,384,64]{2,3,1,0:T(8,128)S(1)} fusion(f32[384,384,4]{1,0,2:T(8,128)} %get-tuple-element.151, f32[4,384]{1,0:T(4,128)S(1)} %bitcast.134, f32[1,4,384,64]{2,3,1,0:T(8,128)S(1)} %get-tuple-element.164, f32[4,384]{1,0:T(4,128)S(1)} %get-tuple-element.152, pred[]{:T(512)S(6)} %compare.18, bf16[384,128]{0,1:T(8,128)(2,1)S(1)} %bitcast.133), kind=kOutput, calls=%fused_computation.9.clone.1 | convolution fusion | flops 77561856 | bytes 3207169 | tf_op jit(solution)/shard_map/while/body/eval_jaxpr/kgqs,skd->kgqd/dot_general | solution.py:76
  121.8 1.9 bitcast_reduce_fusion.2
  123.7 2.4 %fusion.82 = f32[1,4,384,64]{2,3,1,0:T(8,128)S(1)} fusion(f32[384,384,4]{1,0,2:T(8,128)} %get-tuple-element.151, f32[4,384]{1,0:T(4,128)S(1)} %bitcast.134, f32[1,4,384,64]{2,3,1,0:T(8,128)S(1)} %get-tuple-element.164, f32[4,384]{1,0:T(4,128)S(1)} %get-tuple-element.152, pred[]{:T(512)S(6)} %compare.18, bf16[384,128]{0,1:T(8,128)(2,1)S(1)} %bitcast.133), kind=kOutput, calls=%fused_computation.9.clone.1 | convolution fusion | flops 77561856 | bytes 3207169 | tf_op jit(solution)/shard_map/while/body/eval_jaxpr/kgqs,skd->kgqd/dot_general | solution.py:76
  127.8 1.9 bitcast_reduce_fusion.2
  129.8 2.4 %fusion.82 = f32[1,4,384,64]{2,3,1,0:T(8,128)S(1)} fusion(f32[384,384,4]{1,0,2:T(8,128)} %get-tuple-element.151, f32[4,384]{1,0:T(4,128)S(1)} %bitcast.134, f32[1,4,384,64]{2,3,1,0:T(8,128)S(1)} %get-tuple-element.164, f32[4,384]{1,0:T(4,128)S(1)} %get-tuple-element.152, pred[]{:T(512)S(6)} %compare.18, bf16[384,128]{0,1:T(8,128)(2,1)S(1)} %bitcast.133), kind=kOutput, calls=%fused_computation.9.clone.1 | convolution fusion | flops 77561856 | bytes 3207169 | tf_op jit(solution)/shard_map/while/body/eval_jaxpr/kgqs,skd->kgqd/dot_general | solution.py:76
  133.7 1.9 bitcast_reduce_fusion.2
  135.6 2.4 %fusion.82 = f32[1,4,384,64]{2,3,1,0:T(8,128)S(1)} fusion(f32[384,384,4]{1,0,2:T(8,128)} %get-tuple-element.151, f32[4,384]{1,0:T(4,128)S(1)} %bitcast.134, f32[1,4,384,64]{2,3,1,0:T(8,128)S(1)} %get-tuple-element.164, f32[4,384]{1,0:T(4,128)S(1)} %get-tuple-element.152, pred[]{:T(512)S(6)} %compare.18, bf16[384,128]{0,1:T(8,128)(2,1)S(1)} %bitcast.133), kind=kOutput, calls=%fused_computation.9.clone.1 | convolution fusion | flops 77561856 | bytes 3207169 | tf_op jit(solution)/shard_map/while/body/eval_jaxpr/kgqs,skd->kgqd/dot_general | solution.py:76
  139.5 1.9 bitcast_reduce_fusion.2
  141.4 2.4 %fusion.82 = f32[1,4,384,64]{2,3,1,0:T(8,128)S(1)} fusion(f32[384,384,4]{1,0,2:T(8,128)} %get-tuple-element.151, f32[4,384]{1,0:T(4,128)S(1)} %bitcast.134, f32[1,4,384,64]{2,3,1,0:T(8,128)S(1)} %get-tuple-element.164, f32[4,384]{1,0:T(4,128)S(1)} %get-tuple-element.152, pred[]{:T(512)S(6)} %compare.18, bf16[384,128]{0,1:T(8,128)(2,1)S(1)} %bitcast.133), kind=kOutput, calls=%fused_computation.9.clone.1 | convolution fusion | flops 77561856 | bytes 3207169 | tf_op jit(solution)/shard_map/while/body/eval_jaxpr/kgqs,skd->kgqd/dot_general | solution.py:76
  145.3 1.9 bitcast_reduce_fusion.2
  147.2 2.4 %fusion.82 = f32[1,4,384,64]{2,3,1,0:T(8,128)S(1)} fusion(f32[384,384,4]{1,0,2:T(8,128)} %get-tuple-element.151, f32[4,384]{1,0:T(4,128)S(1)} %bitcast.134, f32[1,4,384,64]{2,3,1,0:T(8,128)S(1)} %get-tuple-element.164, f32[4,384]{1,0:T(4,128)S(1)} %get-tuple-element.152, pred[]{:T(512)S(6)} %compare.18, bf16[384,128]{0,1:T(8,128)(2,1)S(1)} %bitcast.133), kind=kOutput, calls=%fused_computation.9.clone.1 | convolution fusion | flops 77561856 | bytes 3207169 | tf_op jit(solution)/shard_map/while/body/eval_jaxpr/kgqs,skd->kgqd/dot_general | solution.py:76
  151.1 1.9 bitcast_reduce_fusion.2
  153.1 2.4 %fusion.82 = f32[1,4,384,64]{2,3,1,0:T(8,128)S(1)} fusion(f32[384,384,4]{1,0,2:T(8,128)} %get-tuple-element.151, f32[4,384]{1,0:T(4,128)S(1)} %bitcast.134, f32[1,4,384,64]{2,3,1,0:T(8,128)S(1)} %get-tuple-element.164, f32[4,384]{1,0:T(4,128)S(1)} %get-tuple-element.152, pred[]{:T(512)S(6)} %compare.18, bf16[384,128]{0,1:T(8,128)(2,1)S(1)} %bitcast.133), kind=kOutput, calls=%fused_computation.9.clone.1 | convolution fusion | flops 77561856 | bytes 3207169 | tf_op jit(solution)/shard_map/while/body/eval_jaxpr/kgqs,skd->kgqd/dot_general | solution.py:76
  155.9 3.0 %bitcast_convert_fusion = bf16[384,2048]{1,0:T(8,128)(2,1)} fusion(bf16[4,64,2048]{2,1,0:T(8,128)(2,1)} %bitcast.144, f32[1,4,384,64]{2,3,1,0:T(8,128)S(1)} %get-tuple-element.35, f32[4,384]{1,0:T(4,128)S(1)} %bitcast.140), kind=kOutput, calls=%fused_computation.40 | convolution fusion | flops 403636224 | bytes 3020800 | tf_op jit(solution)/shard_map/kgqd,kgde->qe/dot_general | solution.py:99
  159.0 2.1 slice.56
  161.0 3.8 %all-to-all-start.1 = ((bf16[8,96,512]{2,1,0:T(8,128)(2,1)}), bf16[8,96,512]{2,1,0:T(8,128)(2,1)S(1)}, u32[]{:S(2)}, u32[]{:S(2)}) async-start(bf16[8,96,512]{2,1,0:T(8,128)(2,1)} %bitcast.137), calls=%async_computation.2 | async-start | bytes 1572864 | tf_op jit(solution)/shard_map/all_to_all | solution.py:176
  165.0 35.9 %all-reduce.2.cloned.1.call-done = bf16[384,2048]{1,0:T(8,128)(2,1)} async-done(((bf16[384,2048]{1,0:T(8,128)(2,1)}), bf16[384,2048]{1,0:T(8,128)(2,1)}) %all-reduce.2.cloned.1.call-update) | async-done | bytes 1572880 | tf_op jit(solution)/shard_map/psum | solution.py:102
  204.5 2.6 %gather_fusion.1 = bf16[512,512]{1,0:T(8,128)(2,1)} fusion(bf16[768,512]{1,0:T(8,128)(2,1)S(1)} %bitcast.131, s32[1024]{0:T(1024)S(1)} %pad_clamp_fusion), kind=kCustom, calls=%fused_computation.1 | custom fusion | bytes 1050624 | tf_op jit(solution)/shard_map/gather | solution.py:177
  (156 shorter events, 31.6 us)
Async XLA Ops:
  7.2 81.0 %copy-start = (bf16[512,2048]{1,0:T(8,128)(2,1)S(1)}, bf16[512,2048]{1,0:T(8,128)(2,1)}, u32[]{:S(2)}) copy-start(bf16[512,2048]{1,0:T(8,128)(2,1)} %param.35) | copy-start | bytes 6291460
  7.2 8.0 %copy-start.3 = (bf16[256,2048]{1,0:T(8,128)(2,1)S(1)}, bf16[256,2048]{1,0:T(8,128)(2,1)}, u32[]{:S(2)}) copy-start(bf16[256,2048]{1,0:T(8,128)(2,1)} %param.26) | copy-start | bytes 3145732
  7.2 85.3 %all-gather.2.cloned.1.call-start = ((), (), s32[]{:S(2)}) async-start(), calls=%async_computation.4 | async-start | bytes 3932160 | tf_op jit(solution)/shard_map/all_gather | solution.py:153
  16.1 1.0 copy-start.4
  19.8 29.0 %copy-start.10 = (f32[64]{0:T(128)S(1)}, f32[64]{0:T(128)}, u32[]{:S(2)}) copy-start(f32[64]{0:T(128)} %param.23) | copy-start | bytes 772
  19.8 29.5 %copy-start.7 = (bf16[384,256]{1,0:T(8,128)(2,1)S(1)}, bf16[384,256]{1,0:T(8,128)(2,1)}, u32[]{:S(2)}) copy-start(bf16[384,256]{1,0:T(8,128)(2,1)} %param.19) | copy-start | bytes 589828
  20.0 29.9 %copy-start.11 = (f32[64]{0:T(128)S(1)}, f32[64]{0:T(128)}, u32[]{:S(2)}) copy-start(f32[64]{0:T(128)} %param.22) | copy-start | bytes 772
  47.4 111.6 %reduce-scatter.2.cloned.1.call-start = ((), (), s32[]{:S(2)}) async-start(), calls=%async_computation.5 | async-start | bytes 5242880 | tf_op jit(solution)/shard_map/reduce_scatter | solution.py:167
  49.5 1.2 copy-start.5
  92.5 6.3 %copy-start.12 = (bf16[1,2048,1024]{2,1,0:T(8,128)(2,1)S(1)}, bf16[1,2048,1024]{2,1,0:T(8,128)(2,1)}, u32[]{:S(2)}) copy-start(bf16[1,2048,1024]{2,1,0:T(8,128)(2,1)} %param.31) | copy-start | bytes 12582916
  92.5 6.3 %copy-start.14 = (bf16[1,768,2048]{2,1,0:T(8,128)(2,1)S(1)}, bf16[1,768,2048]{2,1,0:T(8,128)(2,1)}, u32[]{:S(2)}) copy-start(bf16[1,768,2048]{2,1,0:T(8,128)(2,1)} %all-gather.2.cloned.1.call-done) | copy-start | bytes 9437188
  98.8 3.6 %copy-start.13 = (bf16[1,1024,2048]{2,1,0:T(8,128)(2,1)S(1)}, bf16[1,1024,2048]{2,1,0:T(8,128)(2,1)}, u32[]{:S(2)}) copy-start(bf16[1,1024,2048]{2,1,0:T(8,128)(2,1)} %param.32) | copy-start | bytes 12582916
  102.4 3.6 %copy-start.6 = (bf16[256,2048]{1,0:T(8,128)(2,1)S(1)}, bf16[256,2048]{1,0:T(8,128)(2,1)}, u32[]{:S(2)}) copy-start(bf16[256,2048]{1,0:T(8,128)(2,1)} %convolution_convert_fusion) | copy-start | bytes 3145732
  108.3 92.6 %all-reduce.2.cloned.1.call-start = ((), (), s32[]{:S(2)}) async-start(), calls=%async_computation.3 | async-start | bytes 3145728 | tf_op jit(solution)/shard_map/psum | solution.py:102
  111.3 3.1 %copy-start.1 = (f32[384,384,4]{1,0,2:T(8,128)S(1)}, f32[384,384,4]{1,0,2:T(8,128)}, u32[]{:S(2)}) copy-start(f32[384,384,4]{1,0,2:T(8,128)} %get-tuple-element.151) | copy-start | bytes 7077892 | tf_op jit(solution)/shard_map/while
  117.8 2.5 %copy-start.1 = (f32[384,384,4]{1,0,2:T(8,128)S(1)}, f32[384,384,4]{1,0,2:T(8,128)}, u32[]{:S(2)}) copy-start(f32[384,384,4]{1,0,2:T(8,128)} %get-tuple-element.151) | copy-start | bytes 7077892 | tf_op jit(solution)/shard_map/while
  123.7 2.6 %copy-start.1 = (f32[384,384,4]{1,0,2:T(8,128)S(1)}, f32[384,384,4]{1,0,2:T(8,128)}, u32[]{:S(2)}) copy-start(f32[384,384,4]{1,0,2:T(8,128)} %get-tuple-element.151) | copy-start | bytes 7077892 | tf_op jit(solution)/shard_map/while
  129.7 2.4 %copy-start.1 = (f32[384,384,4]{1,0,2:T(8,128)S(1)}, f32[384,384,4]{1,0,2:T(8,128)}, u32[]{:S(2)}) copy-start(f32[384,384,4]{1,0,2:T(8,128)} %get-tuple-element.151) | copy-start | bytes 7077892 | tf_op jit(solution)/shard_map/while
  135.6 2.4 %copy-start.1 = (f32[384,384,4]{1,0,2:T(8,128)S(1)}, f32[384,384,4]{1,0,2:T(8,128)}, u32[]{:S(2)}) copy-start(f32[384,384,4]{1,0,2:T(8,128)} %get-tuple-element.151) | copy-start | bytes 7077892 | tf_op jit(solution)/shard_map/while
  141.4 2.4 %copy-start.1 = (f32[384,384,4]{1,0,2:T(8,128)S(1)}, f32[384,384,4]{1,0,2:T(8,128)}, u32[]{:S(2)}) copy-start(f32[384,384,4]{1,0,2:T(8,128)} %get-tuple-element.151) | copy-start | bytes 7077892 | tf_op jit(solution)/shard_map/while
  147.2 2.4 %copy-start.1 = (f32[384,384,4]{1,0,2:T(8,128)S(1)}, f32[384,384,4]{1,0,2:T(8,128)}, u32[]{:S(2)}) copy-start(f32[384,384,4]{1,0,2:T(8,128)} %get-tuple-element.151) | copy-start | bytes 7077892 | tf_op jit(solution)/shard_map/while
  153.1 2.4 %copy-start.1 = (f32[384,384,4]{1,0,2:T(8,128)S(1)}, f32[384,384,4]{1,0,2:T(8,128)}, u32[]{:S(2)}) copy-start(f32[384,384,4]{1,0,2:T(8,128)} %get-tuple-element.151) | copy-start | bytes 7077892 | tf_op jit(solution)/shard_map/while
  158.9 5.9 %copy-start.9 = (f32[256,2]{0,1:T(2,128)S(1)}, f32[256,2]{0,1:T(2,128)}, u32[]{:S(2)}) copy-start(f32[256,2]{0,1:T(2,128)} %param.28) | copy-start | bytes 6148
  158.9 43.9 %copy-start.8 = (f32[2048]{0:T(1024)S(1)}, f32[2048]{0:T(1024)}, u32[]{:S(2)}) copy-start(f32[2048]{0:T(1024)} %param.25) | copy-start | bytes 24580
  161.0 43.4 %all-to-all-start.1 = ((bf16[8,96,512]{2,1,0:T(8,128)(2,1)}), bf16[8,96,512]{2,1,0:T(8,128)(2,1)S(1)}, u32[]{:S(2)}, u32[]{:S(2)}) async-start(bf16[8,96,512]{2,1,0:T(8,128)(2,1)} %bitcast.137), calls=%async_computation.2 | async-start | bytes 1572864 | tf_op jit(solution)/shard_map/all_to_all | solution.py:176
  200.9 1.9 copy-start.2
Sparse Core Ops, SparseCore 0:
  47.5 27.5 all-gather.1
  108.4 43.3 reduce-scatter.1
  159.1 41.8 all-reduce.1
where the time goes:
time: 219 us; the launch traced here: 218 us
  blocking collectives  61.6 us (28%)
  matrix products  58.9 us (27%)
  waiting for transfers between devices  36 us (16%)
  local copies, waits for them, and re-layouts  25.5 us (12%)
  other arithmetic  17.9 us (8%)
  between operations  14.2 us (6%)
  starting transfers between devices  3.9 us (2%)
    psum x1, waiting for transfers between devices, mixer_half(): lax.psum(partial_value.astype(jnp.bfloat16), 'tp').astype(jnp.float32)  35.9 us
    all_gather x1, blocking collectives, mixer_half(): piece = lax.all_gather(stacked, 'ep', axis=0, tiled=True)  34.3 us
    all_to_all x1, blocking collectives, expert_half(): lax.all_to_all(outgoing, 'ep', split_axis=0, concat_axis=0, tiled=True)  27.3 us
    dot_general x8, matrix products, step_block(): jnp.einsum('kgqs,skd->kgqd', exponent.astype(jnp.bfloat16), block_values,...  19.6 us
    dot_general x8, matrix products, step_block(): jnp.einsum('qkgd,skd->kgqs', query_grouped, block_keys, preferred_element...  15.3 us
    dynamic_slice x16, local copies, waits for them, and re-layouts, mixer_half(): carry, unused = lax.scan(step_block, carry, blocks)  8.26 us
    dot_general x1, matrix products, expert_half(): jnp.einsum('esd,edf->esf', piece, gate_weight, preferred_element_type=jnp...  6.28 us
  transfers between devices with their start and end apart: 4, of which 1 were waited for; matrix products, arithmetic and copies ran while one was open for 30% of the time, Pallas kernels for 0%

commit v1 on v0

--- a/solution.py
+++ b/solution.py
@@ -99,7 +99,9 @@
     partial_value = jnp.einsum(
         "kgqd,kgde->qe", attended, lane_weight, preferred_element_type=jnp.float32
     )
-    mixer_sum = lax.psum(partial_value.astype(jnp.bfloat16), "tp").astype(jnp.float32)
+    mixer_sum = jnp.sum(lax.all_gather(partial_value.astype(jnp.bfloat16), "tp"), axis=0).astype(
+        jnp.float32
+    )
     mixer_scale = lax.rsqrt(jnp.mean(mixer_sum * mixer_sum, axis=1, keepdims=True) + EPSILON)
     return (mixer_sum * mixer_scale * mixer_gain).astype(jnp.bfloat16)
 

time: 219 us -> 228 us (1.041)
  other arithmetic: 17.9 us -> 23.7 us
  waiting for transfers between devices: 36 us -> 39.5 us
    all_gather x0 -> x1, waiting for transfers between devices: none -> 39.5 us  [mixer_half(): lax.all_gather(partial_value.astype(jnp.bfloat16), 'tp')]
    psum x1 -> x0, waiting for transfers between devices: 35.9 us -> none  [mixer_half(): lax.psum(partial_value.astype(jnp.bfloat16), 'tp').astype(jnp.float32)]
    reduce_sum x0 -> x1, other arithmetic: none -> 5.66 us  [mixer_half(): jnp.sum(lax.all_gather(partial_value.astype(jnp.bfloat16), 'tp'), axis=0)]
  transfers between devices with their start and end apart: 4 -> 4, of which waited for: 1 -> 1; matrix products, arithmetic and copies ran while one was open for 30% -> 31% of each run, Pallas kernels for 0% -> 0%
where the time goes in v1:
time: 228 us
  blocking collectives  61.6 us (27%)
  matrix products  58.8 us (26%)
  waiting for transfers between devices  39.5 us (17%)
  local copies, waits for them, and re-layouts  25.5 us (11%)
  other arithmetic  23.7 us (10%)
  between operations  14.2 us (6%)
  starting transfers between devices  3.91 us (2%)
    all_gather x1, waiting for transfers between devices, mixer_half(): lax.all_gather(partial_value.astype(jnp.bfloat16), 'tp')  39.5 us
    all_gather x1, blocking collectives, mixer_half(): piece = lax.all_gather(stacked, 'ep', axis=0, tiled=True)  34.3 us
    all_to_all x1, blocking collectives, expert_half(): lax.all_to_all(outgoing, 'ep', split_axis=0, concat_axis=0, tiled=True)  27.3 us
    dot_general x8, matrix products, step_block(): jnp.einsum('kgqs,skd->kgqd', exponent.astype(jnp.bfloat16), block_values,...  19.6 us
    dot_general x8, matrix products, step_block(): jnp.einsum('qkgd,skd->kgqs', query_grouped, block_keys, preferred_element...  15.3 us
    dynamic_slice x16, local copies, waits for them, and re-layouts, mixer_half(): carry, unused = lax.scan(step_block, carry, blocks)  8.25 us
    dot_general x1, matrix products, expert_half(): jnp.einsum('esd,edf->esf', piece, gate_weight, preferred_element_type=jnp...  6.28 us
    reduce_sum x1, other arithmetic, mixer_half(): jnp.sum(lax.all_gather(partial_value.astype(jnp.bfloat16), 'tp'), axis=0)  5.66 us
  transfers between devices with their start and end apart: 4, of which 1 were waited for; matrix products, arithmetic and copies ran while one was open for 31% of the time, Pallas kernels for 0%

profile of v1, /device:TPU:0, one launch (start us, length us, event | category | flops | bytes accessed | tf_op | source)
XLA Modules:
  0.0 227.6 jit_solution(15658847584594740488)
XLA Ops:
  11.0 2.4 %scatter_custom_fusion = s32[768]{0:T(1024)S(1)} fusion(s32[512]{0:T(512)S(1)} %bitcast.143, s32[512]{0:T(512)S(1)} %add_select_fusion, s32[]{:T(128)} %constant.117.clone.1), kind=kCustom, calls=%fused_computation.114 | custom fusion | bytes 3076 | tf_op jit(solution)/shard_map/scatter | solution.py:143
  17.1 2.7 %gather_fusion = bf16[768,512]{1,0:T(8,128)(2,1)S(1)} fusion(bf16[256,512]{1,0:T(8,128)(2,1)S(1)} %constant_dynamic-slice_fusion.1, s32[1024]{0:T(1024)S(1)} %pad_clamp_fusion.1), kind=kCustom, calls=%fused_computation | custom fusion | bytes 1575936 | tf_op jit(solution)/shard_map/gather | solution.py:149
  20.0 27.3 %all_to_all.10 = bf16[8,96,512]{2,1,0:T(8,128)(2,1)} all-to-all(bf16[8,96,512]{2,1,0:T(8,128)(2,1)S(1)} %broadcast_select_fusion), channel_id=1, replica_groups=mesh['ep'=8,'tp'=4] {'ep'}, dimensions={0} | all-to-all | bytes 1572864 | tf_op jit(solution)/shard_map/all_to_all | solution.py:152
  50.8 3.1 %fusion.67 = f32[256,512]{1,0:T(8,128)} fusion(bf16[256,2048]{1,0:T(8,128)(2,1)S(1)} %copy-done.5, bf16[2048,512]{1,0:T(8,128)(2,1)} %param.33), kind=kOutput, calls=%fused_computation.131 | convolution fusion | flops 536870912 | bytes 3670016 | tf_op jit(solution)/shard_map/dot_general | solution.py:164
  53.9 34.3 %all_gather.12 = bf16[3072,128]{1,0:T(8,128)(2,1)} all-gather(bf16[384,128]{1,0:T(8,128)(2,1)S(1)} %pad_maximum_fusion.2), channel_id=1, replica_groups=mesh['ep'=8,'tp'=4] {'ep'}, dimensions={0}, use_global_device_ids=true | all-gather | bytes 884736 | tf_op jit(solution)/shard_map/all_gather | solution.py:90
  88.1 4.3 %convolution_convert_fusion = bf16[256,2048]{1,0:T(8,128)(2,1)} fusion(bf16[512,2048]{1,0:T(8,128)(2,1)S(1)} %copy-done, bf16[256,2048]{1,0:T(8,128)(2,1)} %copy-done.4, bf16[2048,512]{1,0:T(8,128)(2,1)} %param.34, f32[256,512]{1,0:T(8,128)} %fusion.67), kind=kOutput, calls=%fused_computation.44 | convolution fusion | flops 1075052544 | bytes 6815744 | tf_op jit(solution)/shard_map/dot_general | solution.py:167
  92.5 6.3 %fusion.16 = f32[768,1024]{1,0:T(8,128)S(1)} fusion(bf16[1,2048,1024]{2,1,0:T(8,128)(2,1)} %param.30, bf16[1,768,2048]{2,1,0:T(8,128)(2,1)} %all-gather.4.cloned.1.call-done), kind=kOutput, calls=%fused_computation.30 | convolution fusion | flops 3221225472 | bytes 10485760 | tf_op jit(solution)/shard_map/esd,edf->esf/dot_general | solution.py:156
  98.8 3.6 %multiply_convert_fusion = bf16[768,1024]{1,0:T(8,128)(2,1)S(1)} fusion(f32[768,1024]{1,0:T(8,128)S(1)} %fusion.16, bf16[1,2048,1024]{2,1,0:T(8,128)(2,1)S(1)} %copy-done.12, bf16[1,768,2048]{2,1,0:T(8,128)(2,1)S(1)} %copy-done.14), kind=kOutput, calls=%fused_computation.41 | convolution fusion | flops 3225944064 | bytes 12058624 | tf_op jit(solution)/shard_map/esd,edf->esf/dot_general | solution.py:157
  102.4 3.6 %fusion.18 = bf16[768,2048]{1,0:T(8,128)(2,1)S(1)} fusion(bf16[768,1024]{1,0:T(8,128)(2,1)S(1)} %multiply_convert_fusion, bf16[1,1024,2048]{2,1,0:T(8,128)(2,1)S(1)} %copy-done.13), kind=kOutput, calls=%fused_computation.34 | convolution fusion | flops 3222798336 | bytes 8912896 | tf_op jit(solution)/shard_map/esf,efd->esd/dot_general | solution.py:159
  106.1 2.3 %pad_maximum_fusion = bf16[1024,2048]{1,0:T(8,128)(2,1)} fusion(bf16[256,2048]{1,0:T(8,128)(2,1)S(1)} %copy-done.6, bf16[768,2048]{1,0:T(8,128)(2,1)S(1)} %fusion.18), kind=kLoop, calls=%fused_computation.25 | loop fusion | flops 8388608 | bytes 8388608 | tf_op jit(solution)/shard_map/concatenate | solution.py:168
  108.5 47.5 %while.15 = (s32[]{:T(128)}, f32[1,4,384]{2,1,0:T(4,128)S(1)}, f32[1,4,384]{2,1,0:T(4,128)S(1)}, f32[1,4,384,64]{2,3,1,0:T(8,128)S(1)}, bf16[8,384,128]{2,1,0:T(...) while((s32[]{:T(128)}, f32[1,4,384]{2,1,0:T(4,128)S(1)}, ...), condition=%wide.region_5.6_spmd.clone, body=%wide.region_2.5_spmd.clone.sunk | while | flops 156017664 | bytes 18088064 | solution.py:95
  109.5 1.9 bitcast_reduce_fusion.2
  111.5 2.8 %fusion.82 = f32[1,4,384,64]{2,3,1,0:T(8,128)S(1)} fusion(f32[384,384,4]{1,0,2:T(8,128)} %get-tuple-element.151, f32[4,384]{1,0:T(4,128)S(1)} %bitcast.136, f32[1,4,384,64]{2,3,1,0:T(8,128)S(1)} %get-tuple-element.164, f32[4,384]{1,0:T(4,128)S(1)} %get-tuple-element.152, pred[]{:T(512)S(6)} %compare.18, bf16[384,128]{0,1:T(8,128)(2,1)S(1)} %bitcast.134), kind=kOutput, calls=%fused_computation.9.clone.1 | convolution fusion | flops 77561856 | bytes 3207169 | tf_op jit(solution)/shard_map/while/body/eval_jaxpr/kgqs,skd->kgqd/dot_general | solution.py:76
  117.9 2.5 %fusion.82 = f32[1,4,384,64]{2,3,1,0:T(8,128)S(1)} fusion(f32[384,384,4]{1,0,2:T(8,128)} %get-tuple-element.151, f32[4,384]{1,0:T(4,128)S(1)} %bitcast.136, f32[1,4,384,64]{2,3,1,0:T(8,128)S(1)} %get-tuple-element.164, f32[4,384]{1,0:T(4,128)S(1)} %get-tuple-element.152, pred[]{:T(512)S(6)} %compare.18, bf16[384,128]{0,1:T(8,128)(2,1)S(1)} %bitcast.134), kind=kOutput, calls=%fused_computation.9.clone.1 | convolution fusion | flops 77561856 | bytes 3207169 | tf_op jit(solution)/shard_map/while/body/eval_jaxpr/kgqs,skd->kgqd/dot_general | solution.py:76
  121.9 1.9 bitcast_reduce_fusion.2
  123.8 2.4 %fusion.82 = f32[1,4,384,64]{2,3,1,0:T(8,128)S(1)} fusion(f32[384,384,4]{1,0,2:T(8,128)} %get-tuple-element.151, f32[4,384]{1,0:T(4,128)S(1)} %bitcast.136, f32[1,4,384,64]{2,3,1,0:T(8,128)S(1)} %get-tuple-element.164, f32[4,384]{1,0:T(4,128)S(1)} %get-tuple-element.152, pred[]{:T(512)S(6)} %compare.18, bf16[384,128]{0,1:T(8,128)(2,1)S(1)} %bitcast.134), kind=kOutput, calls=%fused_computation.9.clone.1 | convolution fusion | flops 77561856 | bytes 3207169 | tf_op jit(solution)/shard_map/while/body/eval_jaxpr/kgqs,skd->kgqd/dot_general | solution.py:76
  127.9 1.9 bitcast_reduce_fusion.2
  129.8 2.4 %fusion.82 = f32[1,4,384,64]{2,3,1,0:T(8,128)S(1)} fusion(f32[384,384,4]{1,0,2:T(8,128)} %get-tuple-element.151, f32[4,384]{1,0:T(4,128)S(1)} %bitcast.136, f32[1,4,384,64]{2,3,1,0:T(8,128)S(1)} %get-tuple-element.164, f32[4,384]{1,0:T(4,128)S(1)} %get-tuple-element.152, pred[]{:T(512)S(6)} %compare.18, bf16[384,128]{0,1:T(8,128)(2,1)S(1)} %bitcast.134), kind=kOutput, calls=%fused_computation.9.clone.1 | convolution fusion | flops 77561856 | bytes 3207169 | tf_op jit(solution)/shard_map/while/body/eval_jaxpr/kgqs,skd->kgqd/dot_general | solution.py:76
  133.7 1.9 bitcast_reduce_fusion.2
  135.6 2.4 %fusion.82 = f32[1,4,384,64]{2,3,1,0:T(8,128)S(1)} fusion(f32[384,384,4]{1,0,2:T(8,128)} %get-tuple-element.151, f32[4,384]{1,0:T(4,128)S(1)} %bitcast.136, f32[1,4,384,64]{2,3,1,0:T(8,128)S(1)} %get-tuple-element.164, f32[4,384]{1,0:T(4,128)S(1)} %get-tuple-element.152, pred[]{:T(512)S(6)} %compare.18, bf16[384,128]{0,1:T(8,128)(2,1)S(1)} %bitcast.134), kind=kOutput, calls=%fused_computation.9.clone.1 | convolution fusion | flops 77561856 | bytes 3207169 | tf_op jit(solution)/shard_map/while/body/eval_jaxpr/kgqs,skd->kgqd/dot_general | solution.py:76
  141.5 2.4 %fusion.82 = f32[1,4,384,64]{2,3,1,0:T(8,128)S(1)} fusion(f32[384,384,4]{1,0,2:T(8,128)} %get-tuple-element.151, f32[4,384]{1,0:T(4,128)S(1)} %bitcast.136, f32[1,4,384,64]{2,3,1,0:T(8,128)S(1)} %get-tuple-element.164, f32[4,384]{1,0:T(4,128)S(1)} %get-tuple-element.152, pred[]{:T(512)S(6)} %compare.18, bf16[384,128]{0,1:T(8,128)(2,1)S(1)} %bitcast.134), kind=kOutput, calls=%fused_computation.9.clone.1 | convolution fusion | flops 77561856 | bytes 3207169 | tf_op jit(solution)/shard_map/while/body/eval_jaxpr/kgqs,skd->kgqd/dot_general | solution.py:76
  145.4 1.9 bitcast_reduce_fusion.2
  147.3 2.4 %fusion.82 = f32[1,4,384,64]{2,3,1,0:T(8,128)S(1)} fusion(f32[384,384,4]{1,0,2:T(8,128)} %get-tuple-element.151, f32[4,384]{1,0:T(4,128)S(1)} %bitcast.136, f32[1,4,384,64]{2,3,1,0:T(8,128)S(1)} %get-tuple-element.164, f32[4,384]{1,0:T(4,128)S(1)} %get-tuple-element.152, pred[]{:T(512)S(6)} %compare.18, bf16[384,128]{0,1:T(8,128)(2,1)S(1)} %bitcast.134), kind=kOutput, calls=%fused_computation.9.clone.1 | convolution fusion | flops 77561856 | bytes 3207169 | tf_op jit(solution)/shard_map/while/body/eval_jaxpr/kgqs,skd->kgqd/dot_general | solution.py:76
  151.2 1.9 bitcast_reduce_fusion.2
  153.1 2.4 %fusion.82 = f32[1,4,384,64]{2,3,1,0:T(8,128)S(1)} fusion(f32[384,384,4]{1,0,2:T(8,128)} %get-tuple-element.151, f32[4,384]{1,0:T(4,128)S(1)} %bitcast.136, f32[1,4,384,64]{2,3,1,0:T(8,128)S(1)} %get-tuple-element.164, f32[4,384]{1,0:T(4,128)S(1)} %get-tuple-element.152, pred[]{:T(512)S(6)} %compare.18, bf16[384,128]{0,1:T(8,128)(2,1)S(1)} %bitcast.134), kind=kOutput, calls=%fused_computation.9.clone.1 | convolution fusion | flops 77561856 | bytes 3207169 | tf_op jit(solution)/shard_map/while/body/eval_jaxpr/kgqs,skd->kgqd/dot_general | solution.py:76
  156.0 3.0 %bitcast_convert_fusion = bf16[384,2048]{1,0:T(8,128)(2,1)} fusion(bf16[4,64,2048]{2,1,0:T(8,128)(2,1)} %bitcast.146, f32[1,4,384,64]{2,3,1,0:T(8,128)S(1)} %get-tuple-element.35, f32[4,384]{1,0:T(4,128)S(1)} %bitcast.142), kind=kOutput, calls=%fused_computation.40 | convolution fusion | flops 403636224 | bytes 3020800 | tf_op jit(solution)/shard_map/kgqd,kgde->qe/dot_general | solution.py:99
  159.0 2.1 slice.56
  161.1 3.8 %all-to-all-start.1 = ((bf16[8,96,512]{2,1,0:T(8,128)(2,1)}), bf16[8,96,512]{2,1,0:T(8,128)(2,1)S(1)}, u32[]{:S(2)}, u32[]{:S(2)}) async-start(bf16[8,96,512]{2,1,0:T(8,128)(2,1)} %bitcast.139), calls=%async_computation.2 | async-start | bytes 1572864 | tf_op jit(solution)/shard_map/all_to_all | solution.py:178
  165.1 39.5 %all-gather.6.cloned.1.call-done = bf16[1536,2048]{1,0:T(8,128)(2,1)} async-done(((bf16[384,2048]{1,0:T(8,128)(2,1)}), bf16[1536,2048]{1,0:T(8,128)(2,1)}) %all-gather.6.cloned.1.call-update) | async-done | bytes 6291472 | tf_op jit(solution)/shard_map/all_gather | solution.py:102
  204.5 5.7 %reduce_sum.90 = bf16[384,2048]{1,0:T(8,128)(2,1)} reduce(bf16[4,384,2048]{2,1,0:T(8,128)(2,1)} %bitcast.135, bf16[]{:T(256)} %constant.129.clone.1), dimensions={0}, to_apply=%region_6.7 | reduce | flops 2359296 | bytes 7864322 | tf_op jit(solution)/shard_map/reduce_sum | solution.py:102
  210.2 1.9 fusion.21
  213.7 2.6 %gather_fusion.1 = bf16[512,512]{1,0:T(8,128)(2,1)} fusion(bf16[768,512]{1,0:T(8,128)(2,1)S(1)} %bitcast.132, s32[1024]{0:T(1024)S(1)} %pad_clamp_fusion), kind=kCustom, calls=%fused_computation.1 | custom fusion | bytes 1050624 | tf_op jit(solution)/shard_map/gather | solution.py:179
  (157 shorter events, 33.5 us)
Async XLA Ops:
  7.2 81.0 %copy-start = (bf16[512,2048]{1,0:T(8,128)(2,1)S(1)}, bf16[512,2048]{1,0:T(8,128)(2,1)}, u32[]{:S(2)}) copy-start(bf16[512,2048]{1,0:T(8,128)(2,1)} %param.35) | copy-start | bytes 6291460
  7.2 8.0 %copy-start.3 = (bf16[256,2048]{1,0:T(8,128)(2,1)S(1)}, bf16[256,2048]{1,0:T(8,128)(2,1)}, u32[]{:S(2)}) copy-start(bf16[256,2048]{1,0:T(8,128)(2,1)} %param.26) | copy-start | bytes 3145732
  7.2 85.3 %all-gather.4.cloned.1.call-start = ((), (), s32[]{:S(2)}) async-start(), calls=%async_computation.3 | async-start | bytes 3932160 | tf_op jit(solution)/shard_map/all_gather | solution.py:155
  16.1 1.0 copy-start.4
  19.8 29.0 %copy-start.10 = (f32[64]{0:T(128)S(1)}, f32[64]{0:T(128)}, u32[]{:S(2)}) copy-start(f32[64]{0:T(128)} %param.23) | copy-start | bytes 772
  19.8 29.5 %copy-start.7 = (bf16[384,256]{1,0:T(8,128)(2,1)S(1)}, bf16[384,256]{1,0:T(8,128)(2,1)}, u32[]{:S(2)}) copy-start(bf16[384,256]{1,0:T(8,128)(2,1)} %param.19) | copy-start | bytes 589828
  20.0 29.9 %copy-start.11 = (f32[64]{0:T(128)S(1)}, f32[64]{0:T(128)}, u32[]{:S(2)}) copy-start(f32[64]{0:T(128)} %param.22) | copy-start | bytes 772
  47.4 111.6 %reduce-scatter.2.cloned.1.call-start = ((), (), s32[]{:S(2)}) async-start(), calls=%async_computation.4 | async-start | bytes 5242880 | tf_op jit(solution)/shard_map/reduce_scatter | solution.py:169
  49.5 1.2 copy-start.5
  92.5 6.3 %copy-start.12 = (bf16[1,2048,1024]{2,1,0:T(8,128)(2,1)S(1)}, bf16[1,2048,1024]{2,1,0:T(8,128)(2,1)}, u32[]{:S(2)}) copy-start(bf16[1,2048,1024]{2,1,0:T(8,128)(2,1)} %param.31) | copy-start | bytes 12582916
  92.5 6.3 %copy-start.14 = (bf16[1,768,2048]{2,1,0:T(8,128)(2,1)S(1)}, bf16[1,768,2048]{2,1,0:T(8,128)(2,1)}, u32[]{:S(2)}) copy-start(bf16[1,768,2048]{2,1,0:T(8,128)(2,1)} %all-gather.4.cloned.1.call-done) | copy-start | bytes 9437188
  98.8 3.6 %copy-start.13 = (bf16[1,1024,2048]{2,1,0:T(8,128)(2,1)S(1)}, bf16[1,1024,2048]{2,1,0:T(8,128)(2,1)}, u32[]{:S(2)}) copy-start(bf16[1,1024,2048]{2,1,0:T(8,128)(2,1)} %param.32) | copy-start | bytes 12582916
  102.4 3.6 %copy-start.6 = (bf16[256,2048]{1,0:T(8,128)(2,1)S(1)}, bf16[256,2048]{1,0:T(8,128)(2,1)}, u32[]{:S(2)}) copy-start(bf16[256,2048]{1,0:T(8,128)(2,1)} %convolution_convert_fusion) | copy-start | bytes 3145732
  108.4 96.1 %all-gather.6.cloned.1.call-start = ((), (), s32[]{:S(2)}) async-start(), calls=%async_computation.5 | async-start | bytes 7864320 | tf_op jit(solution)/shard_map/all_gather | solution.py:102
  111.4 3.1 %copy-start.1 = (f32[384,384,4]{1,0,2:T(8,128)S(1)}, f32[384,384,4]{1,0,2:T(8,128)}, u32[]{:S(2)}) copy-start(f32[384,384,4]{1,0,2:T(8,128)} %get-tuple-element.151) | copy-start | bytes 7077892 | tf_op jit(solution)/shard_map/while
  117.9 2.5 %copy-start.1 = (f32[384,384,4]{1,0,2:T(8,128)S(1)}, f32[384,384,4]{1,0,2:T(8,128)}, u32[]{:S(2)}) copy-start(f32[384,384,4]{1,0,2:T(8,128)} %get-tuple-element.151) | copy-start | bytes 7077892 | tf_op jit(solution)/shard_map/while
  123.8 2.6 %copy-start.1 = (f32[384,384,4]{1,0,2:T(8,128)S(1)}, f32[384,384,4]{1,0,2:T(8,128)}, u32[]{:S(2)}) copy-start(f32[384,384,4]{1,0,2:T(8,128)} %get-tuple-element.151) | copy-start | bytes 7077892 | tf_op jit(solution)/shard_map/while
  129.8 2.4 %copy-start.1 = (f32[384,384,4]{1,0,2:T(8,128)S(1)}, f32[384,384,4]{1,0,2:T(8,128)}, u32[]{:S(2)}) copy-start(f32[384,384,4]{1,0,2:T(8,128)} %get-tuple-element.151) | copy-start | bytes 7077892 | tf_op jit(solution)/shard_map/while
  135.6 2.4 %copy-start.1 = (f32[384,384,4]{1,0,2:T(8,128)S(1)}, f32[384,384,4]{1,0,2:T(8,128)}, u32[]{:S(2)}) copy-start(f32[384,384,4]{1,0,2:T(8,128)} %get-tuple-element.151) | copy-start | bytes 7077892 | tf_op jit(solution)/shard_map/while
  141.4 2.4 %copy-start.1 = (f32[384,384,4]{1,0,2:T(8,128)S(1)}, f32[384,384,4]{1,0,2:T(8,128)}, u32[]{:S(2)}) copy-start(f32[384,384,4]{1,0,2:T(8,128)} %get-tuple-element.151) | copy-start | bytes 7077892 | tf_op jit(solution)/shard_map/while
  147.3 2.4 %copy-start.1 = (f32[384,384,4]{1,0,2:T(8,128)S(1)}, f32[384,384,4]{1,0,2:T(8,128)}, u32[]{:S(2)}) copy-start(f32[384,384,4]{1,0,2:T(8,128)} %get-tuple-element.151) | copy-start | bytes 7077892 | tf_op jit(solution)/shard_map/while
  153.1 2.4 %copy-start.1 = (f32[384,384,4]{1,0,2:T(8,128)S(1)}, f32[384,384,4]{1,0,2:T(8,128)}, u32[]{:S(2)}) copy-start(f32[384,384,4]{1,0,2:T(8,128)} %get-tuple-element.151) | copy-start | bytes 7077892 | tf_op jit(solution)/shard_map/while
  158.9 5.9 %copy-start.9 = (f32[256,2]{0,1:T(2,128)S(1)}, f32[256,2]{0,1:T(2,128)}, u32[]{:S(2)}) copy-start(f32[256,2]{0,1:T(2,128)} %param.28) | copy-start | bytes 6148
  161.1 52.6 %all-to-all-start.1 = ((bf16[8,96,512]{2,1,0:T(8,128)(2,1)}), bf16[8,96,512]{2,1,0:T(8,128)(2,1)S(1)}, u32[]{:S(2)}, u32[]{:S(2)}) async-start(bf16[8,96,512]{2,1,0:T(8,128)(2,1)} %bitcast.139), calls=%async_computation.2 | async-start | bytes 1572864 | tf_op jit(solution)/shard_map/all_to_all | solution.py:178
  204.5 7.6 %copy-start.8 = (f32[2048]{0:T(1024)S(1)}, f32[2048]{0:T(1024)}, u32[]{:S(2)}) copy-start(f32[2048]{0:T(1024)} %param.25) | copy-start | bytes 24580
  210.2 1.9 copy-start.2
Sparse Core Ops, SparseCore 0:
  47.5 27.5 all-gather.3
  108.6 43.3 reduce-scatter.1
  159.1 45.3 all-gather.5
